TPU v7x, 32 devices: a whole 2x2x4 slice. The times are simulated.
32 devices in a mesh: fs: 8 (over z, x), tp: 4 (over y, core).
Axes of the slice: x: 2, y: 2, z: 4, core: 2. Of those that a mesh axis runs over, the one named last changes fastest.
Arguments:
- prompt_tokens: bfloat16 [6144, 2048], P('fs', 'tp'), may hold values from -6 to 6
- norm_gain: float32 [2048], P('fs'), may hold values from 0.1 to 1.9
- up_master: float32 [2048, 4096], P('fs', 'tp'), may hold values from -6 to 6
- down_master: float32 [2048, 4096], P('fs', 'tp'), may hold values from -6 to 6
Outputs:
- serve_up: bfloat16 [2048, 4096], P(None, 'tp')
- serve_down: bfloat16 [2048, 4096], P(None, 'tp')
- mixed: bfloat16 [6144, 2048], P('fs', 'tp')
All inputs are finite; a program needn't handle non-finite values.
Results may differ from a plain program's by a relative error of at most 0.009.
Values may be sent and summed in bfloat16 or wider, within the bound.
A program may use at most 64 MiB of HBM per device.

v0:
```python
import functools

import jax
import jax.numpy as jnp
from jax import lax
from jax.experimental import pallas as pl
from jax.experimental.pallas import tpu as pltpu
from jax.sharding import PartitionSpec as P

MESH = pl.DeviceIdType.MESH
LANES = 128


def plain(prompt_tokens, norm_gain, up_master, down_master):
    up_folded = (norm_gain[:, None] * up_master).astype(jnp.bfloat16)
    down_cast = down_master.astype(jnp.bfloat16)
    whole = lax.all_gather(prompt_tokens, "tp", axis=1, tiled=True)
    width = whole.shape[1]
    hidden_units = up_master.shape[1] * lax.axis_size("tp")
    wide = whole.astype(jnp.float32)
    normed = (wide * lax.rsqrt(jnp.mean(wide * wide, axis=1, keepdims=True) + 1e-05)).astype(
        jnp.bfloat16
    )
    contract = (((1,), (1,)), ((), ()))
    serve_up, serve_down = (
        lax.all_gather(up_folded, "fs", axis=0, tiled=True),
        lax.all_gather(down_cast, "fs", axis=0, tiled=True),
    )
    hidden = jnp.dot(normed, serve_up, preferred_element_type=jnp.float32)
    act = jnp.square(jax.nn.relu(hidden * width ** (-0.5))).astype(jnp.bfloat16)
    product = lax.dot_general(act, serve_down, contract, preferred_element_type=jnp.float32)
    partial_value = (product * hidden_units ** (-0.5)).astype(jnp.bfloat16)
    mixed = lax.psum_scatter(partial_value, "tp", scatter_dimension=1, tiled=True)
    return (serve_up, serve_down, mixed)


def kernel(line, pieces, tok, gain, up, down_hbm, wu, wd, mixed,
           xt, xn, act, part, pbuf, psum, rin_p, rin_y,
           w_send, w_recv, t_send, t_recv, a_send, a_recv, b_send, b_recv, c_send, c_recv,
           o_sem, l_sem, down, d_sem):
    T, dl = tok.shape
    r, F = up.shape
    D = wu.shape[0]
    tp = lax.axis_index("tp")
    fs = lax.axis_index("fs")
    z, x = fs // 2, fs % 2
    core, chip = tp % 2, tp // 2
    partner = tp + 1 - 2 * core
    mirror = (tp + 2) % 4
    diag = (partner + 2) % 4
    has_up, has_dn = z < line - 1, z > 0
    W = (wu, wd)
    nb = dl // LANES
    per = r // LANES
    half = T // 2
    zdev = ((fs + 2, tp), (fs - 2, tp), (fs + 1 - 2 * x, tp))

    own_tok = pltpu.make_async_copy(tok, xt.at[tp], l_sem)
    own_tok.start()
    own_down = pltpu.make_async_copy(down_hbm, down, d_sem)
    own_down.start()

    barrier = pltpu.get_barrier_semaphore()

    def greet(dev):
        pl.semaphore_signal(barrier, inc=1, device_id=dev, device_id_type=MESH)

    for other in (partner, mirror, diag):
        greet((fs, other))
    greet(zdev[2])
    pl.when(has_up)(lambda: greet(zdev[0]))
    pl.when(has_dn)(lambda: greet(zdev[1]))

    base = pl.multiple_of(fs * r, r)
    for i in range(r // LANES):
        rows = slice(i * LANES, (i + 1) * LANES)
        g = jnp.transpose(jnp.broadcast_to(gain[:, rows], (LANES, LANES)))
        for c in range(F // LANES):
            cols = slice(c * LANES, (c + 1) * LANES)
            wu[pl.ds(base + i * LANES, LANES), cols] = (g * up[rows, cols]).astype(jnp.bfloat16)
    links = 4 + has_up.astype(jnp.int32) + has_dn.astype(jnp.int32)
    pl.semaphore_wait(barrier, links)

    def piece(a, s, p, way):
        start, size = pieces[p][0], pieces[p][1]
        ref = W[a].at[pl.ds(pl.multiple_of(s * r + start, 8), size), :]
        return pltpu.make_async_remote_copy(
            src_ref=ref, dst_ref=ref, send_sem=w_send.at[way, a, s, p],
            recv_sem=w_recv.at[a, s, p], device_id=zdev[way], device_id_type=MESH)

    def tok_copy(src, k, slot, to):
        return pltpu.make_async_remote_copy(
            src_ref=src, dst_ref=xt.at[k], send_sem=t_send.at[slot], recv_sem=t_recv.at[k],
            device_id=(fs, to), device_id_type=MESH)

    one = [p for p in range(len(pieces)) if pieces[p][2] == 1]
    two = [p for p in range(len(pieces)) if pieces[p][2] == 2]

    def start(d):
        d.start()

    def wait_send(d):
        d.wait_send()

    def own_z(a, do):
        for p in one + two:
            pl.when(has_up)(lambda: do(piece(a, fs, p, 0)))
            pl.when(has_dn)(lambda: do(piece(a, fs, p, 1)))

    def own_x(a, do):
        for p in two + one:
            do(piece(a, fs, p, 2))

    xs = fs + 1 - 2 * x

    def cross(a, do, wait):
        for p in two:
            if wait:
                piece(a, xs, p, 2).wait_recv()
            pl.when(has_up)(lambda: do(piece(a, xs, p, 0)))
            pl.when(has_dn)(lambda: do(piece(a, xs, p, 1)))

    def place(idx):
        got = jnp.int32(0)
        for i in range(line):
            order = sorted(range(line), key=lambda k: (abs(k - i), -k if i < line / 2 else k))
            for q in range(line):
                got = got + jnp.where((z == i) & (idx == q), jnp.int32(order[q]), jnp.int32(0))
        return got

    def relay(a, idx, do, wait, early=True, late=True):
        zz = place(idx)
        onward_up = (zz < z) & has_up
        onward_dn = (zz > z) & has_dn
        same, cross_s = zz * 2 + x, zz * 2 + 1 - x
        for p in one:
            if not (early if pieces[p][0] < LANES else late):
                continue
            if wait:
                piece(a, same, p, 2).wait_recv()
            pl.when(onward_up)(lambda: do(piece(a, same, p, 0)))
            pl.when(onward_dn)(lambda: do(piece(a, same, p, 1)))
            do(piece(a, same, p, 2))
        for p in two if late else ():
            for s in (same, cross_s):
                if wait:
                    piece(a, s, p, 2).wait_recv()
                pl.when(onward_up)(lambda: do(piece(a, s, p, 0)))
                pl.when(onward_dn)(lambda: do(piece(a, s, p, 1)))

    own_x(0, start)
    own_z(0, start)
    own_tok.wait()
    tok_copy(xt.at[tp], tp, 0, mirror).start()
    tok_copy(xt.at[tp], tp, 1, partner).start()
    own_down.wait()
    wd[pl.ds(base, r), :] = down[...].astype(jnp.bfloat16)
    cross(0, start, True)
    for idx in range(1, line):
        relay(0, jnp.int32(idx), start, True)
        if idx == 1:
            tok_copy(xt.at[mirror], mirror, 0, mirror).wait_recv()
            tok_copy(xt.at[mirror], mirror, 2, partner).start()
    own_z(1, start)
    own_x(1, start)

    tok_copy(xt.at[partner], partner, 1, partner).wait_recv()
    tok_copy(xt.at[diag], diag, 1, partner).wait_recv()
    block = 64

    def norm(i, carry):
        rows = pl.ds(pl.multiple_of(i * block, block), block)
        wide = [xt[k, rows, :].astype(jnp.float32) for k in range(4)]
        sq = wide[0] * wide[0]
        for k in range(1, 4):
            sq = sq + wide[k] * wide[k]
        inv = lax.rsqrt(jnp.sum(sq, axis=1, keepdims=True) * (1.0 / D) + 1e-05)
        for k in range(4):
            xn[rows, k * dl:(k + 1) * dl] = (wide[k] * inv).astype(jnp.bfloat16)
        return carry

    lax.fori_loop(0, T // block, norm, 0)

    cross(1, start, True)
    for idx in range(line):
        s = place(jnp.int32(idx)) * 2 + 1 - x
        for p in one:
            piece(0, s, p, 2).wait_recv()

    mrows = 2 * LANES

    def first(i, carry):
        rows = pl.ds(pl.multiple_of(i * mrows, mrows), mrows)
        hidden = jnp.dot(xn[rows, :], wu[...], preferred_element_type=jnp.float32) * D ** (-0.5)
        hidden = jnp.maximum(hidden, 0.0)
        act[rows, :] = (hidden * hidden).astype(jnp.bfloat16)
        return carry

    lax.fori_loop(0, T // mrows, first, 0)

    scale = (F * 4) ** (-0.5)
    mine = pl.ds(pl.multiple_of(core * half, half), half)
    theirs = pl.ds(pl.multiple_of((1 - core) * half, half), half)
    steps = 2 * per
    inner = has_up & has_dn

    def turn(n):
        idx, j = n // steps, n % steps
        last = idx == line - 1
        return jnp.where(last, j % 2, j // per), jnp.where(last, j // 2, j % per)

    def block_of(n):
        side, h = turn(n)
        s = place(n // steps) * 2 + x + side * (1 - 2 * x)
        return s * per + h

    def owner_of(b):
        o = b // nb
        return o, (o // 2) == chip

    def to_partner(b):
        return pltpu.make_async_remote_copy(
            src_ref=part.at[b], dst_ref=rin_p.at[b % nb], send_sem=a_send.at[b],
            recv_sem=a_recv.at[b % nb], device_id=(fs, partner), device_id_type=MESH)

    def swap(b):
        return pltpu.make_async_remote_copy(
            src_ref=part.at[b, theirs, :], dst_ref=pbuf.at[b], send_sem=b_send.at[b],
            recv_sem=b_recv.at[b], device_id=(fs, partner), device_id_type=MESH)

    def to_owner(b, o):
        return pltpu.make_async_remote_copy(
            src_ref=psum.at[b], dst_ref=rin_y.at[b % nb, mine, :], send_sem=c_send.at[b],
            recv_sem=c_recv.at[b % nb, core], device_id=(fs, o), device_id_type=MESH)

    def second_half(b):
        o, here = owner_of(b)

        @pl.when(jnp.logical_not(here))
        def _():
            swap(b).wait_recv()
            psum[b] = (part[b, mine, :].astype(jnp.float32)
                       + pbuf[b].astype(jnp.float32)).astype(jnp.bfloat16)
            to_owner(b, o).start()

    def body(n, carry):
        idx, j = n // steps, n % steps

        @pl.when((j == per) & (idx + 1 < line))
        def _():
            relay(1, idx + 1, start, True, late=False)

        @pl.when((j == per) & (idx + 1 < line) & (inner | (idx + 2 < line)))
        def _():
            relay(1, idx + 1, start, True, early=False)

        @pl.when((j == steps - 2) & (idx == line - 1) & jnp.logical_not(inner))
        def _():
            relay(1, idx, start, True, early=False)

        side, at = turn(n)
        far = place(idx) * 2 + 1 - x
        for h in range(per):
            @pl.when((side == 1) & (at == h))
            def _():
                for p in one:
                    if pieces[p][0] // LANES == h:
                        piece(1, far, p, 2).wait_recv()
        b = block_of(n)
        rhs = wd[pl.ds(pl.multiple_of(b * LANES, LANES), LANES), :]
        product = lax.dot_general(act[...], rhs, (((1,), (1,)), ((), ())),
                                  preferred_element_type=jnp.float32)
        part[b] = (product * scale).astype(jnp.bfloat16)
        o, here = owner_of(b)

        @pl.when(here & (o != tp))
        def _():
            to_partner(b).start()

        @pl.when(jnp.logical_not(here))
        def _():
            swap(b).start()

        @pl.when(n > 0)
        def _():
            second_half(block_of(n - 1))

        return carry

    total = line * steps
    lax.fori_loop(0, total, body, 0)
    second_half(block_of(jnp.int32(total - 1)))

    for i in range(nb):
        b = tp * nb + i
        to_partner(b).wait_recv()
        for c in range(2):
            pltpu.make_async_remote_copy(
                src_ref=psum.at[b], dst_ref=rin_y.at[i, c * half:(c + 1) * half, :],
                send_sem=c_send.at[b], recv_sem=c_recv.at[i, c],
                device_id=(fs, partner), device_id_type=MESH).wait_recv()
        mixed[:, i * LANES:(i + 1) * LANES] = (
            part[b].astype(jnp.float32) + rin_p[i].astype(jnp.float32)
            + rin_y[i].astype(jnp.float32)).astype(jnp.bfloat16)

    for slot, (k, to) in enumerate(((tp, mirror), (tp, partner), (mirror, partner))):
        tok_copy(xt.at[k], k, slot, to).wait_send()
    for a in range(2):
        own_x(a, wait_send)
        own_z(a, wait_send)
        cross(a, wait_send, False)

    def drain(idx, carry):
        for a in range(2):
            relay(a, idx, wait_send, False)
        return carry

    lax.fori_loop(1, line, drain, 0)

    def drain_sums(b, carry):
        o, here = owner_of(b)

        @pl.when(here & (o != tp))
        def _():
            to_partner(b).wait_send()

        @pl.when(jnp.logical_not(here))
        def _():
            swap(b).wait_send()
            to_owner(b, o).wait_send()

        return carry

    lax.fori_loop(0, D // LANES, drain_sums, 0)


def cut(r):
    across = min(LANES - 16, max(16, r * 5 // 32 // 8 * 8))
    got = []
    for first in range(0, r, LANES):
        rows = LANES if first + LANES < r else LANES - across
        if rows == LANES:
            got += [(first, LANES // 2, 1), (first + LANES // 2, LANES // 2, 1)]
        else:
            got += [(first, rows, 1)]
    return got + [(r - across, across, 2)]


def fused(n_fs, prompt_tokens, norm_gain, up_master, down_master):
    T, dl = prompt_tokens.shape
    r, F = up_master.shape
    D = r * n_fs
    line = n_fs // 2
    pieces = cut(r)
    nblk, nb, half = D // LANES, dl // LANES, T // 2
    bf = jnp.bfloat16
    dma = pltpu.SemaphoreType.DMA
    vmem = pl.BlockSpec(memory_space=pltpu.VMEM)
    hbm = pl.BlockSpec(memory_space=pl.ANY)
    return pl.pallas_call(
        functools.partial(kernel, line, pieces),
        out_shape=(pltpu.VMEM((D, F), bf), pltpu.VMEM((D, F), bf), pltpu.VMEM((T, dl), bf)),
        in_specs=[hbm, vmem, vmem, hbm],
        out_specs=(vmem, vmem, vmem),
        scratch_shapes=[
            pltpu.VMEM((4, T, dl), bf), pltpu.VMEM((T, D), bf), pltpu.VMEM((T, F), bf),
            pltpu.VMEM((nblk, T, LANES), bf), pltpu.VMEM((nblk, half, LANES), bf),
            pltpu.VMEM((nblk, half, LANES), bf),
            pltpu.VMEM((nb, T, LANES), bf), pltpu.VMEM((nb, T, LANES), bf),
            dma((3, 2, n_fs, len(pieces))), dma((2, n_fs, len(pieces))),
            dma((3,)), dma((4,)),
            dma((nblk,)), dma((nb,)), dma((nblk,)), dma((nblk,)), dma((nblk,)), dma((nb, 2)),
            dma((line + 1,)), dma,
            pltpu.VMEM((r, F), jnp.float32), dma,
        ],
        compiler_params=pltpu.CompilerParams(
            collective_id=0, has_side_effects=True, vmem_limit_bytes=55 * 2 ** 20),
    )(prompt_tokens, norm_gain.reshape(1, r), up_master, down_master)


def put(src_a, src_b, src_c, dst_a, dst_b, dst_c, sem):
    copies = []
    for src, dst in ((src_a, dst_a), (src_b, dst_b), (src_c, dst_c)):
        n = 4 if src is not src_c else 1
        rows = src.shape[0] // n
        for i in range(n):
            part = pl.ds(i * rows, rows)
            copies.append(pltpu.make_async_copy(
                src.at[part, :], dst.at[part, :], sem.at[len(copies)]))
    for c in copies:
        c.start()
    for c in copies:
        c.wait()


def written(*arrays):
    hbm = pl.BlockSpec(memory_space=pl.ANY)
    return pl.pallas_call(
        put,
        out_shape=tuple(pltpu.HBM(a.shape, a.dtype) for a in arrays),
        in_specs=[pl.BlockSpec(memory_space=pltpu.VMEM)] * 3,
        out_specs=(pl.BlockSpec(memory_space=pltpu.HBM),) * 3,
        scratch_shapes=[pltpu.SemaphoreType.DMA((9,))],
        compiler_params=pltpu.CompilerParams(vmem_limit_bytes=2 ** 20),
    )(*(pltpu.with_memory_space_constraint(a, pltpu.VMEM) for a in arrays))


def solution(mesh):
    n_fs, n_tp = mesh.shape["fs"], mesh.shape["tp"]

    def shards(prompt_tokens, norm_gain, up_master, down_master):
        T, dl = prompt_tokens.shape
        r = up_master.shape[0]
        fits = (n_tp == 4 and n_fs % 2 == 0 and n_fs >= 6 and r % LANES == 0
                and dl % LANES == 0 and T % (2 * LANES) == 0 and r * n_fs == dl * n_tp)
        if not fits:
            return plain(prompt_tokens, norm_gain, up_master, down_master)
        return written(*fused(n_fs, prompt_tokens, norm_gain, up_master, down_master))

    return jax.shard_map(
        shards,
        mesh=mesh,
        in_specs=(P("fs", "tp"), P("fs"), P("fs", "tp"), P("fs", "tp")),
        out_specs=(P(None, "tp"), P(None, "tp"), P("fs", "tp")),
        check_vma=False,
    )
```

profile of v0, /device:TPU:0, one launch (start us, length us, event | category | flops | bytes accessed | tf_op | source)
XLA Modules:
  0.0 101.5 jit_solution(8824948665410367491)
XLA Ops:
  0.6 97.3 %shard_map.67 = (bf16[2048,1024]{1,0:T(8,128)(2,1)S(1)}, bf16[2048,1024]{1,0:T(8,128)(2,1)S(1)}, bf16[768,512]{1,0:T(8,128)(2,1)S(1)}) custom-call(bf16[768,512]{1,0:T(8,128)(2,1)} %tok.1, f32[1,256]{1,0:T(1,128)} %bitcast.1, f32[256,1024]{1,0:T(8,128)} %up.1, f32[256,1024]{1,0:T(8,128)} %down_hbm.1), custom_call_target="tpu_custom_call" | custom-call | tf_op jit(solution)/shard_map/pallas_call | solution.py:360
  97.9 3.6 %shard_map.68 = (bf16[2048,1024]{1,0:T(8,128)(2,1)}, bf16[2048,1024]{1,0:T(8,128)(2,1)}, bf16[768,512]{1,0:T(8,128)(2,1)}) custom-call(bf16[2048,1024]{1,0:T(8,128)(2,1)S(1)} %get-tuple-element.6.src_a, bf16[2048,1024]{1,0:T(8,128)(2,1)S(1)} %get-tuple-element.7.src_b, bf16[768,512]{1,0:T(8,128)(2,1)S(1)} %get-tuple-element.8.src_c), custom_call_target="tpu_custom_call" | custom-call | tf_op jit(solution)/shard_map/pallas_call | solution.py:398
where the time goes:
time: 102 us; the launch traced here: 101 us
  Pallas kernels  101 us (99%)
    pallas_call x1, Pallas kernels, fused(): pl.pallas_call(functools.partial(kernel, line, pieces), out_shape=(pltpu....  97.3 us
    pallas_call x1, Pallas kernels, written(): pl.pallas_call(put, out_shape=tuple((pltpu.HBM(a.shape, a.dtype) for a in...  3.6 us

commit v1 on v0

--- a/solution.py
+++ b/solution.py
@@ -34,12 +34,12 @@
     return (serve_up, serve_down, mixed)
 
 
-def kernel(line, pieces, tok, gain, up, down_hbm, wu, wd, mixed,
+def kernel(line, pieces, tok, gain_hbm, up_hbm, down_hbm, wu, wd, mixed,
            xt, xn, act, part, pbuf, psum, rin_p, rin_y,
            w_send, w_recv, t_send, t_recv, a_send, a_recv, b_send, b_recv, c_send, c_recv,
-           o_sem, l_sem, down, d_sem):
+           l_sem, up, down, gain, d_sem):
     T, dl = tok.shape
-    r, F = up.shape
+    r, F = up_hbm.shape
     D = wu.shape[0]
     tp = lax.axis_index("tp")
     fs = lax.axis_index("fs")
@@ -49,35 +49,44 @@
     mirror = (tp + 2) % 4
     diag = (partner + 2) % 4
     has_up, has_dn = z < line - 1, z > 0
+    inner = has_up & has_dn
+    outer = jnp.logical_not(inner)
+    low = z < line / 2
     W = (wu, wd)
     nb = dl // LANES
     per = r // LANES
     half = T // 2
     zdev = ((fs + 2, tp), (fs - 2, tp), (fs + 1 - 2 * x, tp))
 
-    own_tok = pltpu.make_async_copy(tok, xt.at[tp], l_sem)
-    own_tok.start()
-    own_down = pltpu.make_async_copy(down_hbm, down, d_sem)
-    own_down.start()
-
     barrier = pltpu.get_barrier_semaphore()
 
     def greet(dev):
         pl.semaphore_signal(barrier, inc=1, device_id=dev, device_id_type=MESH)
 
-    for other in (partner, mirror, diag):
-        greet((fs, other))
     greet(zdev[2])
     pl.when(has_up)(lambda: greet(zdev[0]))
     pl.when(has_dn)(lambda: greet(zdev[1]))
+    for other in (mirror, diag, partner):
+        greet((fs, other))
+
+    loads = [pltpu.make_async_copy(gain_hbm, gain, d_sem.at[0]),
+             pltpu.make_async_copy(up_hbm, up, d_sem.at[1]),
+             pltpu.make_async_copy(down_hbm, down, d_sem.at[2])]
+    own_tok = pltpu.make_async_copy(tok, xt.at[tp], l_sem)
+    for load in loads + [own_tok]:
+        load.start()
 
     base = pl.multiple_of(fs * r, r)
-    for i in range(r // LANES):
+    loads[0].wait()
+    loads[1].wait()
+    for i in range(per):
         rows = slice(i * LANES, (i + 1) * LANES)
         g = jnp.transpose(jnp.broadcast_to(gain[:, rows], (LANES, LANES)))
         for c in range(F // LANES):
             cols = slice(c * LANES, (c + 1) * LANES)
             wu[pl.ds(base + i * LANES, LANES), cols] = (g * up[rows, cols]).astype(jnp.bfloat16)
+    loads[2].wait()
+    wd[pl.ds(base, r), :] = down[...].astype(jnp.bfloat16)
     links = 4 + has_up.astype(jnp.int32) + has_dn.astype(jnp.int32)
     pl.semaphore_wait(barrier, links)
 
@@ -95,6 +104,8 @@
 
     one = [p for p in range(len(pieces)) if pieces[p][2] == 1]
     two = [p for p in range(len(pieces)) if pieces[p][2] == 2]
+    early = [p for p in one if pieces[p][0] < r - LANES]
+    late = [p for p in one if p not in early]
 
     def start(d):
         d.start()
@@ -102,13 +113,13 @@
     def wait_send(d):
         d.wait_send()
 
-    def own_z(a, do):
+    def own_z(a, do, up_cond, dn_cond):
         for p in one + two:
-            pl.when(has_up)(lambda: do(piece(a, fs, p, 0)))
-            pl.when(has_dn)(lambda: do(piece(a, fs, p, 1)))
-
-    def own_x(a, do):
-        for p in two + one:
+            pl.when(up_cond)(lambda: do(piece(a, fs, p, 0)))
+            pl.when(dn_cond)(lambda: do(piece(a, fs, p, 1)))
+
+    def own_x(a, do, which):
+        for p in which:
             do(piece(a, fs, p, 2))
 
     xs = fs + 1 - 2 * x
@@ -120,50 +131,63 @@
             pl.when(has_up)(lambda: do(piece(a, xs, p, 0)))
             pl.when(has_dn)(lambda: do(piece(a, xs, p, 1)))
 
-    def place(idx):
+    def near(i, k):
+        return (abs(k - i), -k if i < line / 2 else k)
+
+    def chip_of(k):
+        return (2 * k * per // nb) // 2
+
+    def pick(table):
         got = jnp.int32(0)
         for i in range(line):
-            order = sorted(range(line), key=lambda k: (abs(k - i), -k if i < line / 2 else k))
-            for q in range(line):
-                got = got + jnp.where((z == i) & (idx == q), jnp.int32(order[q]), jnp.int32(0))
+            for y in range(2):
+                got = got + jnp.where((z == i) & (chip == y), jnp.int32(table(i, y)), jnp.int32(0))
         return got
 
-    def relay(a, idx, do, wait, early=True, late=True):
-        zz = place(idx)
+    order_a = [pick(lambda i, y: sorted(range(line), key=lambda k: near(i, k))[q])
+               for q in range(line)]
+    order_b = [pick(lambda i, y: sorted(range(line), key=lambda k: (
+        k != i, chip_of(k) == y, near(i, k)))[q]) for q in range(line)]
+    own_late = inner & (pick(lambda i, y: int(chip_of(i) == y)) == 1)
+
+    def relay(a, zz, do, wait, ones=(), twos=()):
         onward_up = (zz < z) & has_up
         onward_dn = (zz > z) & has_dn
         same, cross_s = zz * 2 + x, zz * 2 + 1 - x
-        for p in one:
-            if not (early if pieces[p][0] < LANES else late):
-                continue
+        for p in ones:
             if wait:
                 piece(a, same, p, 2).wait_recv()
             pl.when(onward_up)(lambda: do(piece(a, same, p, 0)))
             pl.when(onward_dn)(lambda: do(piece(a, same, p, 1)))
             do(piece(a, same, p, 2))
-        for p in two if late else ():
+        for p in twos:
             for s in (same, cross_s):
                 if wait:
                     piece(a, s, p, 2).wait_recv()
                 pl.when(onward_up)(lambda: do(piece(a, s, p, 0)))
                 pl.when(onward_dn)(lambda: do(piece(a, s, p, 1)))
 
-    own_x(0, start)
-    own_z(0, start)
+    own_x(0, start, two)
+    own_z(0, start, has_up, has_dn)
+    own_x(1, start, two)
+    own_x(0, start, one)
     own_tok.wait()
     tok_copy(xt.at[tp], tp, 0, mirror).start()
     tok_copy(xt.at[tp], tp, 1, partner).start()
-    own_down.wait()
-    wd[pl.ds(base, r), :] = down[...].astype(jnp.bfloat16)
     cross(0, start, True)
+    cross(1, start, True)
+    own_z(1, start, outer & has_up, outer & has_dn)
     for idx in range(1, line):
-        relay(0, jnp.int32(idx), start, True)
-        if idx == 1:
-            tok_copy(xt.at[mirror], mirror, 0, mirror).wait_recv()
-            tok_copy(xt.at[mirror], mirror, 2, partner).start()
-    own_z(1, start)
-    own_x(1, start)
-
+        relay(0, order_a[idx], start, True, one, two)
+        if idx == line - 2:
+            own_z(1, start, inner & low, inner & jnp.logical_not(low))
+            pl.when(outer)(lambda: own_x(1, start, one))
+    pl.when(inner)(lambda: own_x(1, start, one))
+    soon = inner & jnp.logical_not(own_late)
+    own_z(1, start, soon & jnp.logical_not(low), soon & low)
+
+    tok_copy(xt.at[mirror], mirror, 0, mirror).wait_recv()
+    tok_copy(xt.at[mirror], mirror, 2, partner).start()
     tok_copy(xt.at[partner], partner, 1, partner).wait_recv()
     tok_copy(xt.at[diag], diag, 1, partner).wait_recv()
     block = 64
@@ -181,11 +205,10 @@
 
     lax.fori_loop(0, T // block, norm, 0)
 
-    cross(1, start, True)
-    for idx in range(line):
-        s = place(jnp.int32(idx)) * 2 + 1 - x
+    relay(1, order_b[1], start, True, one, two)
+    for q in range(line):
         for p in one:
-            piece(0, s, p, 2).wait_recv()
+            piece(0, order_a[q] * 2 + 1 - x, p, 2).wait_recv()
 
     mrows = 2 * LANES
 
@@ -201,18 +224,22 @@
     scale = (F * 4) ** (-0.5)
     mine = pl.ds(pl.multiple_of(core * half, half), half)
     theirs = pl.ds(pl.multiple_of((1 - core) * half, half), half)
-    steps = 2 * per
-    inner = has_up & has_dn
-
-    def turn(n):
-        idx, j = n // steps, n % steps
-        last = idx == line - 1
-        return jnp.where(last, j % 2, j // per), jnp.where(last, j // 2, j % per)
-
-    def block_of(n):
-        side, h = turn(n)
-        s = place(n // steps) * 2 + x + side * (1 - 2 * x)
-        return s * per + h
+    turns = steps_of(line, per)
+    total = line * 2 * per
+
+    codes = []
+    for n in range(total):
+        (qa, sa, ha), (qb, sb, hb) = turns[0][0][n], turns[1][0][n]
+        zz = jnp.where(inner, order_b[qb], order_b[qa])
+        side = jnp.where(inner, jnp.int32(sb), jnp.int32(sa))
+        h = jnp.where(inner, jnp.int32(hb), jnp.int32(ha))
+        codes.append(((zz * 2 + x + side * (1 - 2 * x)) * per + h) * 2 + side)
+
+    def code_of(n):
+        got = jnp.int32(0)
+        for i in range(total):
+            got = got + jnp.where(n == i, codes[i], jnp.int32(0))
+        return got
 
     def owner_of(b):
         o = b // nb
@@ -243,30 +270,32 @@
                        + pbuf[b].astype(jnp.float32)).astype(jnp.bfloat16)
             to_owner(b, o).start()
 
+    groups = {"early": early, "late": late}
+
+    def event(q, what):
+        if what == "two":
+            relay(1, order_b[q], start, True, (), two)
+        else:
+            relay(1, order_b[q], start, True, groups[what], ())
+
     def body(n, carry):
-        idx, j = n // steps, n % steps
-
-        @pl.when((j == per) & (idx + 1 < line))
-        def _():
-            relay(1, idx + 1, start, True, late=False)
-
-        @pl.when((j == per) & (idx + 1 < line) & (inner | (idx + 2 < line)))
-        def _():
-            relay(1, idx + 1, start, True, early=False)
-
-        @pl.when((j == steps - 2) & (idx == line - 1) & jnp.logical_not(inner))
-        def _():
-            relay(1, idx, start, True, early=False)
-
-        side, at = turn(n)
-        far = place(idx) * 2 + 1 - x
-        for h in range(per):
-            @pl.when((side == 1) & (at == h))
+        for role in range(2):
+            mine_too = inner if role else outer
+            for at, todo in turns[role][1].items():
+                @pl.when((n == at) & mine_too)
+                def _():
+                    for q, what in todo:
+                        event(q, what)
+                    if role and at == turns[1][2]:
+                        own_z(1, start, own_late & jnp.logical_not(low), own_late & low)
+
+        code = code_of(n)
+        b, side = code // 2, code % 2
+        s, h = b // per, b % per
+        for p in one:
+            @pl.when((side == 1) & (h == pieces[p][0] // LANES))
             def _():
-                for p in one:
-                    if pieces[p][0] // LANES == h:
-                        piece(1, far, p, 2).wait_recv()
-        b = block_of(n)
+                piece(1, s, p, 2).wait_recv()
         rhs = wd[pl.ds(pl.multiple_of(b * LANES, LANES), LANES), :]
         product = lax.dot_general(act[...], rhs, (((1,), (1,)), ((), ())),
                                   preferred_element_type=jnp.float32)
@@ -283,15 +312,16 @@
 
         @pl.when(n > 0)
         def _():
-            second_half(block_of(n - 1))
+            second_half(code_of(n - 1) // 2)
 
         return carry
 
-    total = line * steps
     lax.fori_loop(0, total, body, 0)
-    second_half(block_of(jnp.int32(total - 1)))
-
-    for i in range(nb):
+    second_half(codes[total - 1] // 2)
+
+    runs = nb // per if nb % per == 0 else 1
+    for q in range(nb):
+        i = (q % runs + x) % runs * (nb // runs) + q // runs
         b = tp * nb + i
         to_partner(b).wait_recv()
         for c in range(2):
@@ -299,23 +329,25 @@
                 src_ref=psum.at[b], dst_ref=rin_y.at[i, c * half:(c + 1) * half, :],
                 send_sem=c_send.at[b], recv_sem=c_recv.at[i, c],
                 device_id=(fs, partner), device_id_type=MESH).wait_recv()
-        mixed[:, i * LANES:(i + 1) * LANES] = (
+        mixed[:, pl.ds(pl.multiple_of(i * LANES, LANES), LANES)] = (
             part[b].astype(jnp.float32) + rin_p[i].astype(jnp.float32)
             + rin_y[i].astype(jnp.float32)).astype(jnp.bfloat16)
 
     for slot, (k, to) in enumerate(((tp, mirror), (tp, partner), (mirror, partner))):
         tok_copy(xt.at[k], k, slot, to).wait_send()
     for a in range(2):
-        own_x(a, wait_send)
-        own_z(a, wait_send)
+        own_x(a, wait_send, one + two)
+        own_z(a, wait_send, has_up, has_dn)
         cross(a, wait_send, False)
 
-    def drain(idx, carry):
-        for a in range(2):
-            relay(a, idx, wait_send, False)
+    def drain(zz, carry):
+        @pl.when(zz != z)
+        def _():
+            for a in range(2):
+                relay(a, zz, wait_send, False, one, two)
         return carry
 
-    lax.fori_loop(1, line, drain, 0)
+    lax.fori_loop(0, line, drain, 0)
 
     def drain_sums(b, carry):
         o, here = owner_of(b)
@@ -332,6 +364,45 @@
         return carry
 
     lax.fori_loop(0, D // LANES, drain_sums, 0)
+
+
+def steps_of(line, per):
+    last = line - 1
+    blocks, before = [], {}
+
+    def add(q, side, hs):
+        blocks.extend((q, side, h) for h in hs)
+
+    def pass_on(*what):
+        before.setdefault(len(blocks), []).extend(what)
+
+    every, head, tail = range(per), range(per - 1), range(per - 1, per)
+    add(0, 0, every)
+    add(0, 1, every)
+    add(1, 0, every)
+    for q in range(2, line):
+        pass_on((q, "early"))
+        add(q - 1, 1, every)
+        if q < last:
+            pass_on((q, "late"), (q, "two"))
+            add(q, 0, every)
+    add(last, 0, head)
+    pass_on((last, "late"))
+    add(last, 1, head)
+    pass_on((last, "two"))
+    add(last, 0, tail)
+    add(last, 1, tail)
+    end = (blocks, before, max(before))
+
+    blocks, before = [], {}
+    add(0, 0, every)
+    add(1, 0, every)
+    for q in range(2, line):
+        pass_on((q, "early"), (q, "late"), (q, "two"))
+        add(q, 0, every)
+    for q in range(line):
+        add(q, 1, every)
+    return end, (blocks, before, max(before))
 
 
 def cut(r):
@@ -339,10 +410,8 @@
     got = []
     for first in range(0, r, LANES):
         rows = LANES if first + LANES < r else LANES - across
-        if rows == LANES:
-            got += [(first, LANES // 2, 1), (first + LANES // 2, LANES // 2, 1)]
-        else:
-            got += [(first, rows, 1)]
+        lead = rows // 2 if rows == LANES else rows * 5 // 8 // 8 * 8
+        got += [(first, lead, 1), (first + lead, rows - lead, 1)] if lead else [(first, rows, 1)]
     return got + [(r - across, across, 2)]
 
 
@@ -360,7 +429,7 @@
     return pl.pallas_call(
         functools.partial(kernel, line, pieces),
         out_shape=(pltpu.VMEM((D, F), bf), pltpu.VMEM((D, F), bf), pltpu.VMEM((T, dl), bf)),
-        in_specs=[hbm, vmem, vmem, hbm],
+        in_specs=[hbm] * 4,
         out_specs=(vmem, vmem, vmem),
         scratch_shapes=[
             pltpu.VMEM((4, T, dl), bf), pltpu.VMEM((T, D), bf), pltpu.VMEM((T, F), bf),
@@ -370,8 +439,8 @@
             dma((3, 2, n_fs, len(pieces))), dma((2, n_fs, len(pieces))),
             dma((3,)), dma((4,)),
             dma((nblk,)), dma((nb,)), dma((nblk,)), dma((nblk,)), dma((nblk,)), dma((nb, 2)),
-            dma((line + 1,)), dma,
-            pltpu.VMEM((r, F), jnp.float32), dma,
+            dma, pltpu.VMEM((r, F), jnp.float32), pltpu.VMEM((r, F), jnp.float32),
+            pltpu.VMEM((1, r), jnp.float32), dma((3,)),
         ],
         compiler_params=pltpu.CompilerParams(
             collective_id=0, has_side_effects=True, vmem_limit_bytes=55 * 2 ** 20),

time: 102 us -> 100 us (0.980)
  Pallas kernels: 101 us -> 99.2 us
    pallas_call x1, Pallas kernels: 97.3 us -> 95.6 us  [fused(): pl.pallas_call(functools.partial(kernel, line, pieces), out_shape=(pltpu....]
where the time goes in v1:
time: 100 us; the launch traced here: 99.8 us
  Pallas kernels  99.2 us (99%)
    pallas_call x1, Pallas kernels, fused(): pl.pallas_call(functools.partial(kernel, line, pieces), out_shape=(pltpu....  95.6 us
    pallas_call x1, Pallas kernels, written(): pl.pallas_call(put, out_shape=tuple((pltpu.HBM(a.shape, a.dtype) for a in...  3.6 us

profile of v1, /device:TPU:0, one launch (start us, length us, event | category | flops | bytes accessed | tf_op | source)
XLA Modules:
  0.0 99.8 jit_solution(7904324483786383942)
XLA Ops:
  0.6 95.6 %shard_map.67 = (bf16[2048,1024]{1,0:T(8,128)(2,1)S(1)}, bf16[2048,1024]{1,0:T(8,128)(2,1)S(1)}, bf16[768,512]{1,0:T(8,128)(2,1)S(1)}) custom-call(bf16[768,512]{1,0:T(8,128)(2,1)} %tok.1, f32[1,256]{1,0:T(1,128)} %bitcast.1, f32[256,1024]{1,0:T(8,128)} %up_hbm.1, f32[256,1024]{1,0:T(8,128)} %down_hbm.1), custom_call_target="tpu_custom_call" | custom-call | tf_op jit(solution)/shard_map/pallas_call | solution.py:429
  96.2 3.6 %shard_map.68 = (bf16[2048,1024]{1,0:T(8,128)(2,1)}, bf16[2048,1024]{1,0:T(8,128)(2,1)}, bf16[768,512]{1,0:T(8,128)(2,1)}) custom-call(bf16[2048,1024]{1,0:T(8,128)(2,1)S(1)} %get-tuple-element.6.src_a, bf16[2048,1024]{1,0:T(8,128)(2,1)S(1)} %get-tuple-element.7.src_b, bf16[768,512]{1,0:T(8,128)(2,1)S(1)} %get-tuple-element.8.src_c), custom_call_target="tpu_custom_call" | custom-call | tf_op jit(solution)/shard_map/pallas_call | solution.py:467

commit v2 on v1

v2 whole, which is shorter than its diff:
```python
import functools

import jax
import jax.numpy as jnp
from jax import lax
from jax.experimental import pallas as pl
from jax.experimental.pallas import tpu as pltpu
from jax.sharding import PartitionSpec as P

MESH = pl.DeviceIdType.MESH
LANES = 128


def plain(prompt_tokens, norm_gain, up_master, down_master):
    up_folded = (norm_gain[:, None] * up_master).astype(jnp.bfloat16)
    down_cast = down_master.astype(jnp.bfloat16)
    whole = lax.all_gather(prompt_tokens, "tp", axis=1, tiled=True)
    width = whole.shape[1]
    hidden_units = up_master.shape[1] * lax.axis_size("tp")
    wide = whole.astype(jnp.float32)
    normed = (wide * lax.rsqrt(jnp.mean(wide * wide, axis=1, keepdims=True) + 1e-05)).astype(
        jnp.bfloat16
    )
    contract = (((1,), (1,)), ((), ()))
    serve_up, serve_down = (
        lax.all_gather(up_folded, "fs", axis=0, tiled=True),
        lax.all_gather(down_cast, "fs", axis=0, tiled=True),
    )
    hidden = jnp.dot(normed, serve_up, preferred_element_type=jnp.float32)
    act = jnp.square(jax.nn.relu(hidden * width ** (-0.5))).astype(jnp.bfloat16)
    product = lax.dot_general(act, serve_down, contract, preferred_element_type=jnp.float32)
    partial_value = (product * hidden_units ** (-0.5)).astype(jnp.bfloat16)
    mixed = lax.psum_scatter(partial_value, "tp", scatter_dimension=1, tiled=True)
    return (serve_up, serve_down, mixed)


def kernel(line, pieces, tok, gain_hbm, up_hbm, down_hbm, wu, wd, mixed,
           xt, xn, act, part, pbuf, psum, rin_p, rin_y,
           w_send, z_recv, x_recv, xa_recv, xb_recv, t_send, t_recv,
           a_send, a_recv, b_send, b_recv, c_send, c_recv,
           l_sem, up, down, gain, d_sem):
    T, dl = tok.shape
    r, F = up_hbm.shape
    D = wu.shape[0]
    tp = lax.axis_index("tp")
    fs = lax.axis_index("fs")
    z, x = fs // 2, fs % 2
    core, chip = tp % 2, tp // 2
    partner = tp + 1 - 2 * core
    mirror = (tp + 2) % 4
    diag = (partner + 2) % 4
    has_up, has_dn = z < line - 1, z > 0
    inner = has_up & has_dn
    outer = jnp.logical_not(inner)
    low = z < line / 2
    high = jnp.logical_not(low)
    W = (wu, wd)
    nb = dl // LANES
    per = r // LANES
    half = T // 2
    zdev = ((fs + 2, tp), (fs - 2, tp), (fs + 1 - 2 * x, tp))

    barrier = pltpu.get_barrier_semaphore()

    def greet(dev):
        pl.semaphore_signal(barrier, inc=1, device_id=dev, device_id_type=MESH)

    greet(zdev[2])
    pl.when(has_up)(lambda: greet(zdev[0]))
    pl.when(has_dn)(lambda: greet(zdev[1]))
    for other in (mirror, diag, partner):
        greet((fs, other))

    def lane_rows(i):
        return slice(i * LANES, (i + 1) * LANES)

    load_gain = pltpu.make_async_copy(gain_hbm, gain, d_sem.at[per])
    load_up = [pltpu.make_async_copy(up_hbm.at[lane_rows(i), :], up.at[lane_rows(i), :],
                                     d_sem.at[i]) for i in range(per)]
    load_down = pltpu.make_async_copy(down_hbm, down, d_sem.at[per + 1])
    own_tok = pltpu.make_async_copy(tok, xt.at[tp], l_sem)
    for load in [load_gain] + load_up + [own_tok, load_down]:
        load.start()

    base = pl.multiple_of(fs * r, r)

    def fold(i):
        load_up[i].wait()
        rows = lane_rows(i)
        g = jnp.transpose(jnp.broadcast_to(gain[:, rows], (LANES, LANES)))
        for c in range(F // LANES):
            cols = lane_rows(c)
            wu[pl.ds(base + i * LANES, LANES), cols] = (g * up[rows, cols]).astype(jnp.bfloat16)

    one = [p for p in range(len(pieces)) if pieces[p][2] == 1]
    two = [p for p in range(len(pieces)) if pieces[p][2] == 2][0]
    across = pieces[two][1]
    single = r - across

    def block_at(p):
        return pieces[p][0] // LANES

    def rows_of(a, first, size):
        return W[a].at[pl.ds(pl.multiple_of(first, 8), size), :]

    def remote(ref, send_sem, recv_sem, way):
        return pltpu.make_async_remote_copy(
            src_ref=ref, dst_ref=ref, send_sem=send_sem, recv_sem=recv_sem,
            device_id=zdev[way], device_id_type=MESH)

    def piece(a, s, p, way):
        if way < 2:
            recv = z_recv.at[a, s // 2, p]
        elif p == two:
            recv = x_recv.at[a]
        else:
            recv = xb_recv.at[s // 2, block_at(p)] if a else xa_recv
        return remote(rows_of(a, s * r + pieces[p][0], pieces[p][1]), w_send.at[way, a], recv, way)

    def tok_copy(src, k, to):
        return pltpu.make_async_remote_copy(
            src_ref=src, dst_ref=xt.at[k], send_sem=t_send, recv_sem=t_recv.at[k],
            device_id=(fs, to), device_id_type=MESH)

    def send_z(a, s, which, up_cond, dn_cond):
        for p in which:
            pl.when(up_cond)(lambda: piece(a, s, p, 0).start())
            pl.when(dn_cond)(lambda: piece(a, s, p, 1).start())

    def send_x(a, s, which):
        for p in which:
            piece(a, s, p, 2).start()

    xs = fs + 1 - 2 * x

    def near(i, k):
        return (abs(k - i), -k if i < line / 2 else k)

    def chip_of(k):
        return (2 * k * per // nb) // 2

    def pick(table):
        got = jnp.int32(0)
        for i in range(line):
            for y in range(2):
                got = got + jnp.where((z == i) & (chip == y), jnp.int32(table(i, y)), jnp.int32(0))
        return got

    order_a = [pick(lambda i, y: sorted(range(line), key=lambda k: near(i, k))[q])
               for q in range(line)]
    order_b = [pick(lambda i, y: sorted(range(line), key=lambda k: (
        k != i, chip_of(k) == y, near(i, k)))[q]) for q in range(line)]
    own_late = inner & (pick(lambda i, y: int(chip_of(i) == y)) == 1)

    def pass_one(a, zz, p):
        same = zz * 2 + x
        piece(a, same, p, 0).wait_recv()
        send_z(a, same, [p], (zz < z) & has_up, (zz > z) & has_dn)
        send_x(a, same, [p])

    def pass_two(a, zz):
        remote(rows_of(a, zz * 2 * r, 2 * across), w_send.at[0, a], z_recv.at[a, zz, two], 0).wait_recv()
        for s in (zz * 2 + x, zz * 2 + 1 - x):
            send_z(a, s, [two], (zz < z) & has_up, (zz > z) & has_dn)

    def send_two(a, up_cond, dn_cond):
        for s in (fs, xs):
            send_z(a, s, [two], up_cond, dn_cond)

    def forward_tokens():
        tok_copy(xt.at[mirror], mirror, mirror).wait_recv()
        tok_copy(xt.at[mirror], mirror, partner).start()

    load_gain.wait()
    for i in range(per):
        fold(i)
    links = 4 + has_up.astype(jnp.int32) + has_dn.astype(jnp.int32)
    pl.semaphore_wait(barrier, links)
    send_x(0, fs, [two])
    send_z(0, fs, one + [two], has_up, has_dn)
    send_x(0, fs, one)
    own_tok.wait()
    tok_copy(xt.at[tp], tp, mirror).start()
    tok_copy(xt.at[tp], tp, partner).start()
    load_down.wait()
    wd[pl.ds(base, r), :] = down[...].astype(jnp.bfloat16)
    pl.when(inner)(lambda: send_x(1, fs, [two]))
    piece(0, xs, two, 2).wait_recv()
    send_z(0, xs, [two], has_up, has_dn)
    send_z(1, fs, one + [two], outer & has_up, outer & has_dn)
    ahead = jnp.logical_not(own_late)

    for idx in range(1, line):
        for p in one:
            pass_one(0, order_a[idx], p)
        if idx == line - 2:
            @pl.when(outer)
            def _():
                send_x(1, fs, [two])
                forward_tokens()
        if idx == line - 1:
            @pl.when(outer)
            def _():
                send_x(1, fs, FILL[0])

            @pl.when(inner)
            def _():
                send_x(1, fs, one)
                forward_tokens()
        pass_two(0, order_a[idx])
        if idx == line - 2:
            @pl.when(inner)
            def _():
                send_z(1, fs, one, low, high)
                piece(1, xs, two, 2).wait_recv()
                send_two(1, low, high)

    @pl.when(inner)
    def _():
        send_z(1, fs, one, ahead & high, ahead & low)

    @pl.when(outer)
    def _():
        piece(1, xs, two, 2).wait_recv()
        send_z(1, xs, [two], has_up, has_dn)

    tok_copy(xt.at[partner], partner, partner).wait_recv()
    tok_copy(xt.at[diag], diag, partner).wait_recv()
    block = 64

    def norm(i, carry):
        rows = pl.ds(pl.multiple_of(i * block, block), block)
        wide = [xt[k, rows, :].astype(jnp.float32) for k in range(4)]
        sq = wide[0] * wide[0]
        for k in range(1, 4):
            sq = sq + wide[k] * wide[k]
        inv = lax.rsqrt(jnp.sum(sq, axis=1, keepdims=True) * (1.0 / D) + 1e-05)
        for k in range(4):
            xn[rows, k * dl:(k + 1) * dl] = (wide[k] * inv).astype(jnp.bfloat16)
        return carry

    lax.fori_loop(0, T // block, norm, 0)

    for p in one:
        pass_one(1, order_b[1], p)

    @pl.when(outer)
    def _():
        send_x(1, fs, FILL[1])

    @pl.when(inner)
    def _():
        for p in EARLY:
            pass_one(1, order_b[2], p)

    remote(rows_of(0, 0, line * single), w_send.at[2, 0], xa_recv, 2).wait_recv()

    mrows = 2 * LANES

    def first(i, carry):
        rows = pl.ds(pl.multiple_of(i * mrows, mrows), mrows)
        hidden = jnp.dot(xn[rows, :], wu[...], preferred_element_type=jnp.float32) * D ** (-0.5)
        hidden = jnp.maximum(hidden, 0.0)
        act[rows, :] = (hidden * hidden).astype(jnp.bfloat16)
        return carry

    lax.fori_loop(0, T // mrows, first, 0)

    scale = (F * 4) ** (-0.5)
    mine = pl.ds(pl.multiple_of(core * half, half), half)
    theirs = pl.ds(pl.multiple_of((1 - core) * half, half), half)
    total = line * 2 * per

    codes = []
    for n in range(total):
        (qa, sa, ha), (qb, sb, hb) = END[n][0], INNER[n][0]
        zz = jnp.where(inner, order_b[qb], order_b[qa])
        side = jnp.where(inner, jnp.int32(sb), jnp.int32(sa))
        h = jnp.where(inner, jnp.int32(hb), jnp.int32(ha))
        codes.append(((zz * 2 + x + side * (1 - 2 * x)) * per + h) * 2 + side)

    def code_of(n):
        got = jnp.int32(0)
        for i in range(total):
            got = got + jnp.where(n == i, codes[i], jnp.int32(0))
        return got

    def owner_of(b):
        o = b // nb
        return o, (o // 2) == chip

    away = 2 * nb

    def to_partner(b):
        return pltpu.make_async_remote_copy(
            src_ref=part.at[b], dst_ref=rin_p.at[b % nb], send_sem=a_send,
            recv_sem=a_recv.at[b % nb], device_id=(fs, partner), device_id_type=MESH)

    def swap(b):
        return pltpu.make_async_remote_copy(
            src_ref=part.at[b, theirs, :], dst_ref=pbuf.at[b % away], send_sem=b_send,
            recv_sem=b_recv.at[b % away], device_id=(fs, partner), device_id_type=MESH)

    def to_owner(b, o):
        return pltpu.make_async_remote_copy(
            src_ref=psum.at[b % away], dst_ref=rin_y.at[b % nb, mine, :], send_sem=c_send,
            recv_sem=c_recv.at[b % nb], device_id=(fs, o), device_id_type=MESH)

    def second_half(b):
        o, here = owner_of(b)

        @pl.when(jnp.logical_not(here))
        def _():
            swap(b).wait_recv()
            psum[b % away] = (part[b, mine, :].astype(jnp.float32)
                              + pbuf[b % away].astype(jnp.float32)).astype(jnp.bfloat16)
            to_owner(b, o).start()

    def event(q, what):
        if what == "two":
            pass_two(1, order_b[q])
        elif what == "fill":
            send_x(1, fs, FILL[2])
        elif what == "own":
            send_z(1, fs, one, own_late & high, own_late & low)
            send_two(1, own_late & high, own_late & low)
        elif what == "own two":
            send_two(1, ahead & high, ahead & low)
        else:
            pass_one(1, order_b[q], what)

    def body(n, carry):
        for here, table in ((outer, END), (inner, INNER)):
            @pl.when(here)
            def _():
                for at in range(total):
                    if table[at][1]:
                        @pl.when(n == at)
                        def _():
                            for q, what in table[at][1]:
                                event(q, what)

        code = code_of(n)
        b, side = code // 2, code % 2
        s, h = b // per, b % per

        @pl.when(side == 1)
        def _():
            for i in range(per):
                size = sum(pieces[p][1] for p in one if block_at(p) == i)
                pl.when(h == i)(lambda: remote(
                    rows_of(1, s * r + i * LANES, size), w_send.at[2, 1],
                    xb_recv.at[s // 2, i], 2).wait_recv())

        rhs = wd[pl.ds(pl.multiple_of(b * LANES, LANES), LANES), :]
        product = lax.dot_general(act[...], rhs, (((1,), (1,)), ((), ())),
                                  preferred_element_type=jnp.float32)
        part[b] = (product * scale).astype(jnp.bfloat16)
        o, here = owner_of(b)

        @pl.when(here & (o != tp))
        def _():
            to_partner(b).start()

        @pl.when(jnp.logical_not(here))
        def _():
            swap(b).start()

        @pl.when(n > 0)
        def _():
            second_half(code_of(n - 1) // 2)

        return carry

    lax.fori_loop(0, total, body, 0)
    second_half(codes[total - 1] // 2)

    runs = nb // per if nb % per == 0 else 1
    for q in range(nb):
        i = (q % runs + x) % runs * (nb // runs) + q // runs
        b = tp * nb + i
        to_partner(b).wait_recv()
        pltpu.make_async_remote_copy(
            src_ref=part.at[b], dst_ref=rin_y.at[i], send_sem=c_send, recv_sem=c_recv.at[i],
            device_id=(fs, partner), device_id_type=MESH).wait_recv()
        mixed[:, pl.ds(pl.multiple_of(i * LANES, LANES), LANES)] = (
            part[b].astype(jnp.float32) + rin_p[i].astype(jnp.float32)
            + rin_y[i].astype(jnp.float32)).astype(jnp.bfloat16)

    def drain(ref, sem):
        pltpu.make_async_remote_copy(
            src_ref=ref, dst_ref=ref, send_sem=sem, recv_sem=l_sem,
            device_id=(fs, partner), device_id_type=MESH).wait_send()

    drain(xt.at[0:3], t_send)
    for a in range(2):
        drain(rows_of(a, 0, r + (line - 1) * single), w_send.at[2, a])
        for i in range(line):
            @pl.when(z == i)
            def _():
                if i < line - 1:
                    drain(rows_of(a, 0, (i + 1) * (r + across)), w_send.at[0, a])
                if i > 0:
                    drain(rows_of(a, 0, (line - i) * (r + across)), w_send.at[1, a])
    drain(part.at[0:nb], a_send)
    drain(pbuf, b_send)
    drain(psum, c_send)


END = (
    ((0, 0, 0), ((2, 0),)), ((0, 0, 1), ()),
    ((1, 0, 0), ((2, 1),)), ((1, 1, 0), ()),
    ((2, 0, 0), ((2, 2), (2, 3), (0, "fill"))),
    ((1, 0, 1), ((1, "two"),)), ((1, 1, 1), ()), ((2, 1, 0), ()),
    ((2, 0, 1), ((2, "two"),)), ((2, 1, 1), ()),
    ((0, 1, 0), ((3, 0),)), ((3, 0, 0), ((3, 1),)), ((0, 1, 1), ()),
    ((3, 1, 0), ((3, 2), (3, 3))), ((3, 0, 1), ((3, "two"),)), ((3, 1, 1), ()),
)
INNER = (
    ((0, 0, 0), ((2, 2), (2, 3), (1, "two"), (0, "own two"))), ((0, 0, 1), ()),
    ((1, 0, 0), ()), ((1, 0, 1), ()),
    ((2, 0, 0), ((2, "two"),)), ((2, 0, 1), ()),
    ((0, 1, 0), ()), ((0, 1, 1), ()),
    ((1, 1, 0), ((3, 0), (3, 1))), ((1, 1, 1), ()),
    ((3, 0, 0), ((3, 2), (3, 3), (3, "two"), (0, "own"))), ((3, 0, 1), ()),
    ((2, 1, 0), ()), ((2, 1, 1), ()), ((3, 1, 0), ()), ((3, 1, 1), ()),
)
EARLY = (0, 1)
FILL = ((0,), (3,), (1, 2))


def cut(r):
    across = r * 5 // 32 // 8 * 8
    lead = (LANES - across) * 5 // 8 // 8 * 8
    h = LANES // 2
    return [(0, h, 1), (h, h, 1), (LANES, lead, 1),
            (LANES + lead, LANES - across - lead, 1), (r - across, across, 2)]


def fused(n_fs, prompt_tokens, norm_gain, up_master, down_master):
    T, dl = prompt_tokens.shape
    r, F = up_master.shape
    D = r * n_fs
    line = n_fs // 2
    pieces = cut(r)
    nblk, nb, half = D // LANES, dl // LANES, T // 2
    bf = jnp.bfloat16
    dma = pltpu.SemaphoreType.DMA
    vmem = pl.BlockSpec(memory_space=pltpu.VMEM)
    hbm = pl.BlockSpec(memory_space=pl.ANY)
    return pl.pallas_call(
        functools.partial(kernel, line, pieces),
        out_shape=(pltpu.VMEM((D, F), bf), pltpu.VMEM((D, F), bf), pltpu.VMEM((T, dl), bf)),
        in_specs=[hbm] * 4,
        out_specs=(vmem, vmem, vmem),
        scratch_shapes=[
            pltpu.VMEM((4, T, dl), bf), pltpu.VMEM((T, D), bf), pltpu.VMEM((T, F), bf),
            pltpu.VMEM((nblk, T, LANES), bf), pltpu.VMEM((2 * nb, half, LANES), bf),
            pltpu.VMEM((2 * nb, half, LANES), bf),
            pltpu.VMEM((nb, T, LANES), bf), pltpu.VMEM((nb, T, LANES), bf),
            dma((3, 2)), dma((2, line, len(pieces))), dma((2,)), dma, dma((line, r // LANES)),
            dma, dma((4,)),
            dma, dma((nb,)), dma, dma((2 * nb,)), dma, dma((nb,)),
            dma, pltpu.VMEM((r, F), jnp.float32), pltpu.VMEM((r, F), jnp.float32),
            pltpu.VMEM((1, r), jnp.float32), dma((r // LANES + 2,)),
        ],
        compiler_params=pltpu.CompilerParams(
            collective_id=0, has_side_effects=True, vmem_limit_bytes=55 * 2 ** 20),
    )(prompt_tokens, norm_gain.reshape(1, r), up_master, down_master)


def put(src_a, src_b, src_c, dst_a, dst_b, dst_c, sem):
    copies = []
    for src, dst in ((src_a, dst_a), (src_b, dst_b), (src_c, dst_c)):
        n = 4 if src is not src_c else 1
        rows = src.shape[0] // n
        for i in range(n):
            part = pl.ds(i * rows, rows)
            copies.append(pltpu.make_async_copy(
                src.at[part, :], dst.at[part, :], sem.at[len(copies)]))
    for c in copies:
        c.start()
    for c in copies:
        c.wait()


def written(*arrays):
    hbm = pl.BlockSpec(memory_space=pl.ANY)
    return pl.pallas_call(
        put,
        out_shape=tuple(pltpu.HBM(a.shape, a.dtype) for a in arrays),
        in_specs=[pl.BlockSpec(memory_space=pltpu.VMEM)] * 3,
        out_specs=(pl.BlockSpec(memory_space=pltpu.HBM),) * 3,
        scratch_shapes=[pltpu.SemaphoreType.DMA((9,))],
        compiler_params=pltpu.CompilerParams(vmem_limit_bytes=2 ** 20),
    )(*(pltpu.with_memory_space_constraint(a, pltpu.VMEM) for a in arrays))


def solution(mesh):
    n_fs, n_tp = mesh.shape["fs"], mesh.shape["tp"]

    def shards(prompt_tokens, norm_gain, up_master, down_master):
        T, dl = prompt_tokens.shape
        r = up_master.shape[0]
        fits = (n_tp == 4 and n_fs == 8 and r == 2 * LANES
                and dl % LANES == 0 and T % (2 * LANES) == 0 and r * n_fs == dl * n_tp)
        if not fits:
            return plain(prompt_tokens, norm_gain, up_master, down_master)
        return written(*fused(n_fs, prompt_tokens, norm_gain, up_master, down_master))

    return jax.shard_map(
        shards,
        mesh=mesh,
        in_specs=(P("fs", "tp"), P("fs"), P("fs", "tp"), P("fs", "tp")),
        out_specs=(P(None, "tp"), P(None, "tp"), P("fs", "tp")),
        check_vma=False,
    )
```

time: 100 us -> 92.5 us (0.925)
  Pallas kernels: 99.2 us -> 91.7 us
    pallas_call x1, Pallas kernels: 95.6 us -> 88.1 us  [fused(): pl.pallas_call(functools.partial(kernel, line, pieces), out_shape=(pltpu....]
where the time goes in v2:
time: 92.5 us; the launch traced here: 92.4 us
  Pallas kernels  91.7 us (99%)
    pallas_call x1, Pallas kernels, fused(): pl.pallas_call(functools.partial(kernel, line, pieces), out_shape=(pltpu....  88.1 us
    pallas_call x1, Pallas kernels, written(): pl.pallas_call(put, out_shape=tuple((pltpu.HBM(a.shape, a.dtype) for a in...  3.6 us

profile of v2, /device:TPU:0, one launch (start us, length us, event | category | flops | bytes accessed | tf_op | source)
XLA Modules:
  0.0 92.4 jit_solution(8188671344845965693)
XLA Ops:
  0.6 88.1 %shard_map.67 = (bf16[2048,1024]{1,0:T(8,128)(2,1)S(1)}, bf16[2048,1024]{1,0:T(8,128)(2,1)S(1)}, bf16[768,512]{1,0:T(8,128)(2,1)S(1)}) custom-call(bf16[768,512]{1,0:T(8,128)(2,1)} %tok.1, f32[1,256]{1,0:T(1,128)} %bitcast.1, f32[256,1024]{1,0:T(8,128)} %up_hbm.1, f32[256,1024]{1,0:T(8,128)} %down_hbm.1), custom_call_target="tpu_custom_call" | custom-call | tf_op jit(solution)/shard_map/pallas_call | solution.py:451
  88.8 3.6 %shard_map.68 = (bf16[2048,1024]{1,0:T(8,128)(2,1)}, bf16[2048,1024]{1,0:T(8,128)(2,1)}, bf16[768,512]{1,0:T(8,128)(2,1)}) custom-call(bf16[2048,1024]{1,0:T(8,128)(2,1)S(1)} %get-tuple-element.6.src_a, bf16[2048,1024]{1,0:T(8,128)(2,1)S(1)} %get-tuple-element.7.src_b, bf16[768,512]{1,0:T(8,128)(2,1)S(1)} %get-tuple-element.8.src_c), custom_call_target="tpu_custom_call" | custom-call | tf_op jit(solution)/shard_map/pallas_call | solution.py:489

commit v3 on v2

--- a/solution.py
+++ b/solution.py
@@ -71,34 +71,41 @@
     for other in (mirror, diag, partner):
         greet((fs, other))
 
+    parts = len(pieces[0])
+    one, two = list(range(parts - 1)), parts - 1
+
     def lane_rows(i):
         return slice(i * LANES, (i + 1) * LANES)
 
-    load_gain = pltpu.make_async_copy(gain_hbm, gain, d_sem.at[per])
-    load_up = [pltpu.make_async_copy(up_hbm.at[lane_rows(i), :], up.at[lane_rows(i), :],
-                                     d_sem.at[i]) for i in range(per)]
-    load_down = pltpu.make_async_copy(down_hbm, down, d_sem.at[per + 1])
+    load_gain = pltpu.make_async_copy(gain_hbm, gain, d_sem.at[parts])
+    def piece_rows(p):
+        return slice(pieces[0][p][0], sum(pieces[0][p]))
+
+    load_up = [pltpu.make_async_copy(up_hbm.at[piece_rows(p), :], up.at[piece_rows(p), :],
+                                     d_sem.at[p]) for p in range(parts)]
+    load_down = pltpu.make_async_copy(down_hbm, down, d_sem.at[parts + 1])
     own_tok = pltpu.make_async_copy(tok, xt.at[tp], l_sem)
-    for load in [load_gain] + load_up + [own_tok, load_down]:
+    for load in [load_gain] + [load_up[p] for p in [two] + one] + [own_tok, load_down]:
         load.start()
 
     base = pl.multiple_of(fs * r, r)
 
-    def fold(i):
-        load_up[i].wait()
-        rows = lane_rows(i)
-        g = jnp.transpose(jnp.broadcast_to(gain[:, rows], (LANES, LANES)))
+    def gains(i):
+        return jnp.transpose(jnp.broadcast_to(gain[:, lane_rows(i)], (LANES, LANES)))
+
+    def fold(p):
+        load_up[p].wait()
+        at, size = pieces[0][p]
+        g = column[at // LANES][at % LANES:at % LANES + size]
         for c in range(F // LANES):
             cols = lane_rows(c)
-            wu[pl.ds(base + i * LANES, LANES), cols] = (g * up[rows, cols]).astype(jnp.bfloat16)
-
-    one = [p for p in range(len(pieces)) if pieces[p][2] == 1]
-    two = [p for p in range(len(pieces)) if pieces[p][2] == 2][0]
-    across = pieces[two][1]
-    single = r - across
+            wu[pl.ds(pl.multiple_of(base + at, 8), size), cols] = (
+                g * up[at:at + size, cols]).astype(jnp.bfloat16)
+
+    across = [pieces[a][two][1] for a in range(2)]
 
     def block_at(p):
-        return pieces[p][0] // LANES
+        return pieces[1][p][0] // LANES
 
     def rows_of(a, first, size):
         return W[a].at[pl.ds(pl.multiple_of(first, 8), size), :]
@@ -110,12 +117,12 @@
 
     def piece(a, s, p, way):
         if way < 2:
-            recv = z_recv.at[a, s // 2, p]
+            recv = z_recv.at[a, (s // 2 - z + (2, 0)[way]) % line, p]
         elif p == two:
             recv = x_recv.at[a]
         else:
             recv = xb_recv.at[s // 2, block_at(p)] if a else xa_recv
-        return remote(rows_of(a, s * r + pieces[p][0], pieces[p][1]), w_send.at[way, a], recv, way)
+        return remote(rows_of(a, s * r + pieces[a][p][0], pieces[a][p][1]), w_send.at[way, a], recv, way)
 
     def tok_copy(src, k, to):
         return pltpu.make_async_remote_copy(
@@ -152,14 +159,18 @@
         k != i, chip_of(k) == y, near(i, k)))[q]) for q in range(line)]
     own_late = inner & (pick(lambda i, y: int(chip_of(i) == y)) == 1)
 
+    def arrived(a, zz, p, first, size):
+        remote(rows_of(a, first, size), w_send.at[0, a],
+               z_recv.at[a, (zz - z + line - 1) % line, p], 0).wait_recv()
+
     def pass_one(a, zz, p):
         same = zz * 2 + x
-        piece(a, same, p, 0).wait_recv()
+        arrived(a, zz, p, same * r + pieces[a][p][0], pieces[a][p][1])
         send_z(a, same, [p], (zz < z) & has_up, (zz > z) & has_dn)
         send_x(a, same, [p])
 
     def pass_two(a, zz):
-        remote(rows_of(a, zz * 2 * r, 2 * across), w_send.at[0, a], z_recv.at[a, zz, two], 0).wait_recv()
+        arrived(a, zz, two, zz * 2 * r, 2 * across[a])
         for s in (zz * 2 + x, zz * 2 + 1 - x):
             send_z(a, s, [two], (zz < z) & has_up, (zz > z) & has_dn)
 
@@ -172,13 +183,18 @@
         tok_copy(xt.at[mirror], mirror, partner).start()
 
     load_gain.wait()
-    for i in range(per):
-        fold(i)
+    column = [gains(i) for i in range(per)]
     links = 4 + has_up.astype(jnp.int32) + has_dn.astype(jnp.int32)
+    fold(two)
+    fold(one[0])
     pl.semaphore_wait(barrier, links)
     send_x(0, fs, [two])
-    send_z(0, fs, one + [two], has_up, has_dn)
-    send_x(0, fs, one)
+    for p in one:
+        if p != one[0]:
+            fold(p)
+        send_z(0, fs, [p], has_up, has_dn)
+        send_x(0, fs, [p])
+    send_z(0, fs, [two], has_up, has_dn)
     own_tok.wait()
     tok_copy(xt.at[tp], tp, mirror).start()
     tok_copy(xt.at[tp], tp, partner).start()
@@ -253,7 +269,7 @@
         for p in EARLY:
             pass_one(1, order_b[2], p)
 
-    remote(rows_of(0, 0, line * single), w_send.at[2, 0], xa_recv, 2).wait_recv()
+    remote(rows_of(0, 0, line * (r - across[0])), w_send.at[2, 0], xa_recv, 2).wait_recv()
 
     mrows = 2 * LANES
 
@@ -262,6 +278,8 @@
         hidden = jnp.dot(xn[rows, :], wu[...], preferred_element_type=jnp.float32) * D ** (-0.5)
         hidden = jnp.maximum(hidden, 0.0)
         act[rows, :] = (hidden * hidden).astype(jnp.bfloat16)
+        for k, p in enumerate(BETWEEN):
+            pl.when(inner & (i == min(k, T // mrows - 1)))(lambda: pass_one(1, order_b[2], p))
         return carry
 
     lax.fori_loop(0, T // mrows, first, 0)
@@ -347,7 +365,7 @@
         @pl.when(side == 1)
         def _():
             for i in range(per):
-                size = sum(pieces[p][1] for p in one if block_at(p) == i)
+                size = sum(pieces[1][p][1] for p in one if block_at(p) == i)
                 pl.when(h == i)(lambda: remote(
                     rows_of(1, s * r + i * LANES, size), w_send.at[2, 1],
                     xb_recv.at[s // 2, i], 2).wait_recv())
@@ -394,14 +412,14 @@
 
     drain(xt.at[0:3], t_send)
     for a in range(2):
-        drain(rows_of(a, 0, r + (line - 1) * single), w_send.at[2, a])
+        drain(rows_of(a, 0, r + (line - 1) * (r - across[a])), w_send.at[2, a])
         for i in range(line):
             @pl.when(z == i)
             def _():
                 if i < line - 1:
-                    drain(rows_of(a, 0, (i + 1) * (r + across)), w_send.at[0, a])
+                    drain(rows_of(a, 0, (i + 1) * (r + across[a])), w_send.at[0, a])
                 if i > 0:
-                    drain(rows_of(a, 0, (line - i) * (r + across)), w_send.at[1, a])
+                    drain(rows_of(a, 0, (line - i) * (r + across[a])), w_send.at[1, a])
     drain(part.at[0:nb], a_send)
     drain(pbuf, b_send)
     drain(psum, c_send)
@@ -412,29 +430,29 @@
     ((1, 0, 0), ((2, 1),)), ((1, 1, 0), ()),
     ((2, 0, 0), ((2, 2), (2, 3), (0, "fill"))),
     ((1, 0, 1), ((1, "two"),)), ((1, 1, 1), ()), ((2, 1, 0), ()),
-    ((2, 0, 1), ((2, "two"),)), ((2, 1, 1), ()),
-    ((0, 1, 0), ((3, 0),)), ((3, 0, 0), ((3, 1),)), ((0, 1, 1), ()),
+    ((2, 0, 1), ((2, "two"),)), ((2, 1, 1), ((3, 0),)),
+    ((0, 1, 0), ()), ((0, 1, 1), ((3, 1),)), ((3, 0, 0), ()),
     ((3, 1, 0), ((3, 2), (3, 3))), ((3, 0, 1), ((3, "two"),)), ((3, 1, 1), ()),
 )
 INNER = (
-    ((0, 0, 0), ((2, 2), (2, 3), (1, "two"), (0, "own two"))), ((0, 0, 1), ()),
+    ((0, 0, 0), ((1, "two"), (0, "own two"))), ((0, 0, 1), ()),
     ((1, 0, 0), ()), ((1, 0, 1), ()),
-    ((2, 0, 0), ((2, "two"),)), ((2, 0, 1), ()),
-    ((0, 1, 0), ()), ((0, 1, 1), ()),
-    ((1, 1, 0), ((3, 0), (3, 1))), ((1, 1, 1), ()),
-    ((3, 0, 0), ((3, 2), (3, 3), (3, "two"), (0, "own"))), ((3, 0, 1), ()),
+    ((2, 0, 0), ((2, "two"), (0, "own"))), ((2, 0, 1), ()),
+    ((0, 1, 0), ((3, 0), (3, 1))), ((0, 1, 1), ((3, 2),)),
+    ((1, 1, 0), ((3, 3),)), ((1, 1, 1), ()),
+    ((3, 0, 0), ((3, "two"),)), ((3, 0, 1), ()),
     ((2, 1, 0), ()), ((2, 1, 1), ()), ((3, 1, 0), ()), ((3, 1, 1), ()),
 )
 EARLY = (0, 1)
-FILL = ((0,), (3,), (1, 2))
-
-
-def cut(r):
-    across = r * 5 // 32 // 8 * 8
-    lead = (LANES - across) * 5 // 8 // 8 * 8
+BETWEEN = (2, 3)
+FILL = ((), (0, 1), (2, 3))
+
+
+def cut(r, share):
+    across = r * share // 32 // 8 * 8
+    lead = (LANES - across) * 21 // 32 // 8 * 8
     h = LANES // 2
-    return [(0, h, 1), (h, h, 1), (LANES, lead, 1),
-            (LANES + lead, LANES - across - lead, 1), (r - across, across, 2)]
+    return [(0, h), (h, h), (LANES, lead), (LANES + lead, LANES - across - lead), (r - across, across)]
 
 
 def fused(n_fs, prompt_tokens, norm_gain, up_master, down_master):
@@ -442,7 +460,7 @@
     r, F = up_master.shape
     D = r * n_fs
     line = n_fs // 2
-    pieces = cut(r)
+    pieces = (cut(r, 3), cut(r, 7))
     nblk, nb, half = D // LANES, dl // LANES, T // 2
     bf = jnp.bfloat16
     dma = pltpu.SemaphoreType.DMA
@@ -458,11 +476,11 @@
             pltpu.VMEM((nblk, T, LANES), bf), pltpu.VMEM((2 * nb, half, LANES), bf),
             pltpu.VMEM((2 * nb, half, LANES), bf),
             pltpu.VMEM((nb, T, LANES), bf), pltpu.VMEM((nb, T, LANES), bf),
-            dma((3, 2)), dma((2, line, len(pieces))), dma((2,)), dma, dma((line, r // LANES)),
+            dma((3, 2)), dma((2, line - 1, len(pieces[0]))), dma((2,)), dma, dma((line, r // LANES)),
             dma, dma((4,)),
             dma, dma((nb,)), dma, dma((2 * nb,)), dma, dma((nb,)),
             dma, pltpu.VMEM((r, F), jnp.float32), pltpu.VMEM((r, F), jnp.float32),
-            pltpu.VMEM((1, r), jnp.float32), dma((r // LANES + 2,)),
+            pltpu.VMEM((1, r), jnp.float32), dma((len(pieces[0]) + 2,)),
         ],
         compiler_params=pltpu.CompilerParams(
             collective_id=0, has_side_effects=True, vmem_limit_bytes=55 * 2 ** 20),

time: 92.5 us -> 91.6 us (level)
  no operation moved by 1% of the time
where the time goes in v3:
time: 91.6 us; the launch traced here: 91.5 us
  Pallas kernels  90.8 us (99%)
    pallas_call x1, Pallas kernels, fused(): pl.pallas_call(functools.partial(kernel, line, pieces), out_shape=(pltpu....  87.2 us
    pallas_call x1, Pallas kernels, written(): pl.pallas_call(put, out_shape=tuple((pltpu.HBM(a.shape, a.dtype) for a in...  3.6 us

profile of v3, /device:TPU:0, one launch (start us, length us, event | category | flops | bytes accessed | tf_op | source)
XLA Modules:
  0.0 91.5 jit_solution(1667754776256629206)
XLA Ops:
  0.6 87.2 %shard_map.67 = (bf16[2048,1024]{1,0:T(8,128)(2,1)S(1)}, bf16[2048,1024]{1,0:T(8,128)(2,1)S(1)}, bf16[768,512]{1,0:T(8,128)(2,1)S(1)}) custom-call(bf16[768,512]{1,0:T(8,128)(2,1)} %tok.1, f32[1,256]{1,0:T(1,128)} %bitcast.1, f32[256,1024]{1,0:T(8,128)} %up_hbm.1, f32[256,1024]{1,0:T(8,128)} %down_hbm.1), custom_call_target="tpu_custom_call" | custom-call | tf_op jit(solution)/shard_map/pallas_call | solution.py:469
  87.9 3.6 %shard_map.68 = (bf16[2048,1024]{1,0:T(8,128)(2,1)}, bf16[2048,1024]{1,0:T(8,128)(2,1)}, bf16[768,512]{1,0:T(8,128)(2,1)}) custom-call(bf16[2048,1024]{1,0:T(8,128)(2,1)S(1)} %get-tuple-element.6.src_a, bf16[2048,1024]{1,0:T(8,128)(2,1)S(1)} %get-tuple-element.7.src_b, bf16[768,512]{1,0:T(8,128)(2,1)S(1)} %get-tuple-element.8.src_c), custom_call_target="tpu_custom_call" | custom-call | tf_op jit(solution)/shard_map/pallas_call | solution.py:507

commit v4 on v3

--- a/solution.py
+++ b/solution.py
@@ -117,7 +117,8 @@
 
     def piece(a, s, p, way):
         if way < 2:
-            recv = z_recv.at[a, (s // 2 - z + (2, 0)[way]) % line, p]
+            recv = z_recv.at[a, (s // 2 - z + (2, 0)[way]) % line,
+                             two + (s + x) % 2 if p == two else p]
         elif p == two:
             recv = x_recv.at[a]
         else:
@@ -169,9 +170,10 @@
         send_z(a, same, [p], (zz < z) & has_up, (zz > z) & has_dn)
         send_x(a, same, [p])
 
-    def pass_two(a, zz):
-        arrived(a, zz, two, zz * 2 * r, 2 * across[a])
-        for s in (zz * 2 + x, zz * 2 + 1 - x):
+    def pass_two(a, zz, sides=(0, 1)):
+        for side in sides:
+            s = zz * 2 + (1 - x if side else x)
+            arrived(a, zz, two + side, s * r + pieces[a][two][0], across[a])
             send_z(a, s, [two], (zz < z) & has_up, (zz > z) & has_dn)
 
     def send_two(a, up_cond, dn_cond):
@@ -289,13 +291,16 @@
     theirs = pl.ds(pl.multiple_of((1 - core) * half, half), half)
     total = line * 2 * per
 
+    keeper = outer & (2 * z * per // nb == tp)
+    roles = ((outer & jnp.logical_not(keeper), END), (keeper, KEEPER), (inner, INNER))
     codes = []
     for n in range(total):
-        (qa, sa, ha), (qb, sb, hb) = END[n][0], INNER[n][0]
-        zz = jnp.where(inner, order_b[qb], order_b[qa])
-        side = jnp.where(inner, jnp.int32(sb), jnp.int32(sa))
-        h = jnp.where(inner, jnp.int32(hb), jnp.int32(ha))
-        codes.append(((zz * 2 + x + side * (1 - 2 * x)) * per + h) * 2 + side)
+        code = jnp.int32(0)
+        for here, table in roles:
+            q, side, h = table[n][0]
+            s = order_b[q] * 2 + (x if side == 0 else 1 - x)
+            code = code + jnp.where(here, (s * per + h) * 2 + side, jnp.int32(0))
+        codes.append(code)
 
     def code_of(n):
         got = jnp.int32(0)
@@ -337,8 +342,12 @@
     def event(q, what):
         if what == "two":
             pass_two(1, order_b[q])
+        elif what == "same":
+            pass_two(1, order_b[q], (0,))
+        elif what == "cross":
+            pass_two(1, order_b[q], (1,))
         elif what == "fill":
-            send_x(1, fs, FILL[2])
+            send_x(1, fs, q)
         elif what == "own":
             send_z(1, fs, one, own_late & high, own_late & low)
             send_two(1, own_late & high, own_late & low)
@@ -348,7 +357,7 @@
             pass_one(1, order_b[q], what)
 
     def body(n, carry):
-        for here, table in ((outer, END), (inner, INNER)):
+        for here, table in roles:
             @pl.when(here)
             def _():
                 for at in range(total):
@@ -428,11 +437,21 @@
 END = (
     ((0, 0, 0), ((2, 0),)), ((0, 0, 1), ()),
     ((1, 0, 0), ((2, 1),)), ((1, 1, 0), ()),
-    ((2, 0, 0), ((2, 2), (2, 3), (0, "fill"))),
+    ((2, 0, 0), ((2, 2), (2, 3), ((2, 3), "fill"))),
     ((1, 0, 1), ((1, "two"),)), ((1, 1, 1), ()), ((2, 1, 0), ()),
     ((2, 0, 1), ((2, "two"),)), ((2, 1, 1), ((3, 0),)),
     ((0, 1, 0), ()), ((0, 1, 1), ((3, 1),)), ((3, 0, 0), ()),
-    ((3, 1, 0), ((3, 2), (3, 3))), ((3, 0, 1), ((3, "two"),)), ((3, 1, 1), ()),
+    ((3, 1, 0), ((3, 2), (3, 3))), ((3, 0, 1), ((3, "same"),)), ((3, 1, 1), ((3, "cross"),)),
+)
+KEEPER = (
+    ((0, 0, 0), ((2, 0),)), ((0, 0, 1), ()),
+    ((1, 0, 0), ((2, 1),)), ((1, 1, 0), ()),
+    ((2, 0, 0), ((2, 2), (2, 3), ((2,), "fill"))),
+    ((1, 0, 1), ((1, "two"),)), ((1, 1, 1), ()), ((2, 1, 0), ()),
+    ((2, 0, 1), ((2, "two"),)), ((2, 1, 1), ((3, 0),)),
+    ((0, 1, 0), ()), ((3, 0, 0), ((3, 1),)),
+    ((3, 1, 0), ((3, 2), (3, 3), ((3,), "fill"))), ((3, 0, 1), ((3, "same"),)), ((3, 1, 1), ((3, "cross"),)),
+    ((0, 1, 1), ()),
 )
 INNER = (
     ((0, 0, 0), ((1, "two"), (0, "own two"))), ((0, 0, 1), ()),
@@ -476,7 +495,7 @@
             pltpu.VMEM((nblk, T, LANES), bf), pltpu.VMEM((2 * nb, half, LANES), bf),
             pltpu.VMEM((2 * nb, half, LANES), bf),
             pltpu.VMEM((nb, T, LANES), bf), pltpu.VMEM((nb, T, LANES), bf),
-            dma((3, 2)), dma((2, line - 1, len(pieces[0]))), dma((2,)), dma, dma((line, r // LANES)),
+            dma((3, 2)), dma((2, line - 1, len(pieces[0]) + 1)), dma((2,)), dma, dma((line, r // LANES)),
             dma, dma((4,)),
             dma, dma((nb,)), dma, dma((2 * nb,)), dma, dma((nb,)),
             dma, pltpu.VMEM((r, F), jnp.float32), pltpu.VMEM((r, F), jnp.float32),

time: 91.6 us -> 91.1 us (level)
  no operation moved by 1% of the time
where the time goes in v4:
time: 91.1 us; the launch traced here: 91 us
  Pallas kernels  90.3 us (99%)
    pallas_call x1, Pallas kernels, fused(): pl.pallas_call(functools.partial(kernel, line, pieces), out_shape=(pltpu....  86.7 us
    pallas_call x1, Pallas kernels, written(): pl.pallas_call(put, out_shape=tuple((pltpu.HBM(a.shape, a.dtype) for a in...  3.6 us

profile of v4, /device:TPU:0, one launch (start us, length us, event | category | flops | bytes accessed | tf_op | source)
XLA Modules:
  0.0 91.0 jit_solution(4479988078211492181)
XLA Ops:
  0.6 86.7 %shard_map.67 = (bf16[2048,1024]{1,0:T(8,128)(2,1)S(1)}, bf16[2048,1024]{1,0:T(8,128)(2,1)S(1)}, bf16[768,512]{1,0:T(8,128)(2,1)S(1)}) custom-call(bf16[768,512]{1,0:T(8,128)(2,1)} %tok.1, f32[1,256]{1,0:T(1,128)} %bitcast.1, f32[256,1024]{1,0:T(8,128)} %up_hbm.1, f32[256,1024]{1,0:T(8,128)} %down_hbm.1), custom_call_target="tpu_custom_call" | custom-call | tf_op jit(solution)/shard_map/pallas_call | solution.py:488
  87.4 3.6 %shard_map.68 = (bf16[2048,1024]{1,0:T(8,128)(2,1)}, bf16[2048,1024]{1,0:T(8,128)(2,1)}, bf16[768,512]{1,0:T(8,128)(2,1)}) custom-call(bf16[2048,1024]{1,0:T(8,128)(2,1)S(1)} %get-tuple-element.6.src_a, bf16[2048,1024]{1,0:T(8,128)(2,1)S(1)} %get-tuple-element.7.src_b, bf16[768,512]{1,0:T(8,128)(2,1)S(1)} %get-tuple-element.8.src_c), custom_call_target="tpu_custom_call" | custom-call | tf_op jit(solution)/shard_map/pallas_call | solution.py:526

commit v5 on v4

--- a/solution.py
+++ b/solution.py
@@ -77,15 +77,11 @@
     def lane_rows(i):
         return slice(i * LANES, (i + 1) * LANES)
 
-    load_gain = pltpu.make_async_copy(gain_hbm, gain, d_sem.at[parts])
-    def piece_rows(p):
-        return slice(pieces[0][p][0], sum(pieces[0][p]))
-
-    load_up = [pltpu.make_async_copy(up_hbm.at[piece_rows(p), :], up.at[piece_rows(p), :],
-                                     d_sem.at[p]) for p in range(parts)]
-    load_down = pltpu.make_async_copy(down_hbm, down, d_sem.at[parts + 1])
+    load_gain = pltpu.make_async_copy(gain_hbm, gain, d_sem.at[1])
+    load_up = pltpu.make_async_copy(up_hbm, up, d_sem.at[0])
+    load_down = pltpu.make_async_copy(down_hbm, down, d_sem.at[2])
     own_tok = pltpu.make_async_copy(tok, xt.at[tp], l_sem)
-    for load in [load_gain] + [load_up[p] for p in [two] + one] + [own_tok, load_down]:
+    for load in (load_gain, load_up, own_tok, load_down):
         load.start()
 
     base = pl.multiple_of(fs * r, r)
@@ -94,7 +90,6 @@
         return jnp.transpose(jnp.broadcast_to(gain[:, lane_rows(i)], (LANES, LANES)))
 
     def fold(p):
-        load_up[p].wait()
         at, size = pieces[0][p]
         g = column[at // LANES][at % LANES:at % LANES + size]
         for c in range(F // LANES):
@@ -186,6 +181,7 @@
 
     load_gain.wait()
     column = [gains(i) for i in range(per)]
+    load_up.wait()
     links = 4 + has_up.astype(jnp.int32) + has_dn.astype(jnp.int32)
     fold(two)
     fold(one[0])
@@ -339,6 +335,19 @@
                               + pbuf[b % away].astype(jnp.float32)).astype(jnp.bfloat16)
             to_owner(b, o).start()
 
+    runs = nb // per if nb % per == 0 else 1
+
+    def finish(q):
+        i = (q % runs + x) % runs * (nb // runs) + q // runs
+        b = tp * nb + i
+        to_partner(b).wait_recv()
+        pltpu.make_async_remote_copy(
+            src_ref=part.at[b], dst_ref=rin_y.at[i], send_sem=c_send, recv_sem=c_recv.at[i],
+            device_id=(fs, partner), device_id_type=MESH).wait_recv()
+        mixed[:, pl.ds(pl.multiple_of(i * LANES, LANES), LANES)] = (
+            part[b].astype(jnp.float32) + rin_p[i].astype(jnp.float32)
+            + rin_y[i].astype(jnp.float32)).astype(jnp.bfloat16)
+
     def event(q, what):
         if what == "two":
             pass_two(1, order_b[q])
@@ -367,6 +376,11 @@
                             for q, what in table[at][1]:
                                 event(q, what)
 
+        @pl.when(keeper & (n == total - 2))
+        def _():
+            for q in range(nb - 1):
+                finish(q)
+
         code = code_of(n)
         b, side = code // 2, code % 2
         s, h = b // per, b % per
@@ -402,17 +416,12 @@
     lax.fori_loop(0, total, body, 0)
     second_half(codes[total - 1] // 2)
 
-    runs = nb // per if nb % per == 0 else 1
-    for q in range(nb):
-        i = (q % runs + x) % runs * (nb // runs) + q // runs
-        b = tp * nb + i
-        to_partner(b).wait_recv()
-        pltpu.make_async_remote_copy(
-            src_ref=part.at[b], dst_ref=rin_y.at[i], send_sem=c_send, recv_sem=c_recv.at[i],
-            device_id=(fs, partner), device_id_type=MESH).wait_recv()
-        mixed[:, pl.ds(pl.multiple_of(i * LANES, LANES), LANES)] = (
-            part[b].astype(jnp.float32) + rin_p[i].astype(jnp.float32)
-            + rin_y[i].astype(jnp.float32)).astype(jnp.bfloat16)
+    @pl.when(jnp.logical_not(keeper))
+    def _():
+        for q in range(nb - 1):
+            finish(q)
+
+    finish(nb - 1)
 
     def drain(ref, sem):
         pltpu.make_async_remote_copy(
@@ -499,7 +508,7 @@
             dma, dma((4,)),
             dma, dma((nb,)), dma, dma((2 * nb,)), dma, dma((nb,)),
             dma, pltpu.VMEM((r, F), jnp.float32), pltpu.VMEM((r, F), jnp.float32),
-            pltpu.VMEM((1, r), jnp.float32), dma((len(pieces[0]) + 2,)),
+            pltpu.VMEM((1, r), jnp.float32), dma((3,)),
         ],
         compiler_params=pltpu.CompilerParams(
             collective_id=0, has_side_effects=True, vmem_limit_bytes=55 * 2 ** 20),

time: 91.1 us -> 91 us (level)
  no operation moved by 1% of the time
where the time goes in v5:
time: 91 us; the launch traced here: 90.8 us
  Pallas kernels  90.2 us (99%)
    pallas_call x1, Pallas kernels, fused(): pl.pallas_call(functools.partial(kernel, line, pieces), out_shape=(pltpu....  86.5 us
    pallas_call x1, Pallas kernels, written(): pl.pallas_call(put, out_shape=tuple((pltpu.HBM(a.shape, a.dtype) for a in...  3.6 us

profile of v5, /device:TPU:0, one launch (start us, length us, event | category | flops | bytes accessed | tf_op | source)
XLA Modules:
  0.0 90.8 jit_solution(16676944212998140561)
XLA Ops:
  0.6 86.5 %shard_map.67 = (bf16[2048,1024]{1,0:T(8,128)(2,1)S(1)}, bf16[2048,1024]{1,0:T(8,128)(2,1)S(1)}, bf16[768,512]{1,0:T(8,128)(2,1)S(1)}) custom-call(bf16[768,512]{1,0:T(8,128)(2,1)} %tok.1, f32[1,256]{1,0:T(1,128)} %bitcast.1, f32[256,1024]{1,0:T(8,128)} %up_hbm.1, f32[256,1024]{1,0:T(8,128)} %down_hbm.1), custom_call_target="tpu_custom_call" | custom-call | tf_op jit(solution)/shard_map/pallas_call | solution.py:497
  87.2 3.6 %shard_map.68 = (bf16[2048,1024]{1,0:T(8,128)(2,1)}, bf16[2048,1024]{1,0:T(8,128)(2,1)}, bf16[768,512]{1,0:T(8,128)(2,1)}) custom-call(bf16[2048,1024]{1,0:T(8,128)(2,1)S(1)} %get-tuple-element.6.src_a, bf16[2048,1024]{1,0:T(8,128)(2,1)S(1)} %get-tuple-element.7.src_b, bf16[768,512]{1,0:T(8,128)(2,1)S(1)} %get-tuple-element.8.src_c), custom_call_target="tpu_custom_call" | custom-call | tf_op jit(solution)/shard_map/pallas_call | solution.py:535

commit v6 on v5

--- a/solution.py
+++ b/solution.py
@@ -195,13 +195,13 @@
     send_z(0, fs, [two], has_up, has_dn)
     own_tok.wait()
     tok_copy(xt.at[tp], tp, mirror).start()
-    tok_copy(xt.at[tp], tp, partner).start()
     load_down.wait()
     wd[pl.ds(base, r), :] = down[...].astype(jnp.bfloat16)
     pl.when(inner)(lambda: send_x(1, fs, [two]))
     piece(0, xs, two, 2).wait_recv()
     send_z(0, xs, [two], has_up, has_dn)
     send_z(1, fs, one + [two], outer & has_up, outer & has_dn)
+    tok_copy(xt.at[tp], tp, partner).start()
     ahead = jnp.logical_not(own_late)
 
     for idx in range(1, line):

time: 91 us -> 91 us (level)
  no operation moved by 1% of the time
where the time goes in v6:
time: 91 us; the launch traced here: 90.8 us
  Pallas kernels  90.2 us (99%)
    pallas_call x1, Pallas kernels, fused(): pl.pallas_call(functools.partial(kernel, line, pieces), out_shape=(pltpu....  86.5 us
    pallas_call x1, Pallas kernels, written(): pl.pallas_call(put, out_shape=tuple((pltpu.HBM(a.shape, a.dtype) for a in...  3.6 us

profile of v6, /device:TPU:0, one launch (start us, length us, event | category | flops | bytes accessed | tf_op | source)
XLA Modules:
  0.0 90.8 jit_solution(706133535674829759)
XLA Ops:
  0.6 86.5 %shard_map.67 = (bf16[2048,1024]{1,0:T(8,128)(2,1)S(1)}, bf16[2048,1024]{1,0:T(8,128)(2,1)S(1)}, bf16[768,512]{1,0:T(8,128)(2,1)S(1)}) custom-call(bf16[768,512]{1,0:T(8,128)(2,1)} %tok.1, f32[1,256]{1,0:T(1,128)} %bitcast.1, f32[256,1024]{1,0:T(8,128)} %up_hbm.1, f32[256,1024]{1,0:T(8,128)} %down_hbm.1), custom_call_target="tpu_custom_call" | custom-call | tf_op jit(solution)/shard_map/pallas_call | solution.py:497
  87.2 3.6 %shard_map.68 = (bf16[2048,1024]{1,0:T(8,128)(2,1)}, bf16[2048,1024]{1,0:T(8,128)(2,1)}, bf16[768,512]{1,0:T(8,128)(2,1)}) custom-call(bf16[2048,1024]{1,0:T(8,128)(2,1)S(1)} %get-tuple-element.6.src_a, bf16[2048,1024]{1,0:T(8,128)(2,1)S(1)} %get-tuple-element.7.src_b, bf16[768,512]{1,0:T(8,128)(2,1)S(1)} %get-tuple-element.8.src_c), custom_call_target="tpu_custom_call" | custom-call | tf_op jit(solution)/shard_map/pallas_call | solution.py:535

commit v7 on v5

--- a/solution.py
+++ b/solution.py
@@ -473,7 +473,7 @@
 )
 EARLY = (0, 1)
 BETWEEN = (2, 3)
-FILL = ((), (0, 1), (2, 3))
+FILL = ((0,), (1,))
 
 
 def cut(r, share):

time: 91 us -> 91 us (level)
  no operation moved by 1% of the time
where the time goes in v7:
time: 91 us; the launch traced here: 90.8 us
  Pallas kernels  90.2 us (99%)
    pallas_call x1, Pallas kernels, fused(): pl.pallas_call(functools.partial(kernel, line, pieces), out_shape=(pltpu....  86.5 us
    pallas_call x1, Pallas kernels, written(): pl.pallas_call(put, out_shape=tuple((pltpu.HBM(a.shape, a.dtype) for a in...  3.6 us

profile of v7, /device:TPU:0, one launch (start us, length us, event | category | flops | bytes accessed | tf_op | source)
XLA Modules:
  0.0 90.8 jit_solution(5525640840271304982)
XLA Ops:
  0.6 86.5 %shard_map.67 = (bf16[2048,1024]{1,0:T(8,128)(2,1)S(1)}, bf16[2048,1024]{1,0:T(8,128)(2,1)S(1)}, bf16[768,512]{1,0:T(8,128)(2,1)S(1)}) custom-call(bf16[768,512]{1,0:T(8,128)(2,1)} %tok.1, f32[1,256]{1,0:T(1,128)} %bitcast.1, f32[256,1024]{1,0:T(8,128)} %up_hbm.1, f32[256,1024]{1,0:T(8,128)} %down_hbm.1), custom_call_target="tpu_custom_call" | custom-call | tf_op jit(solution)/shard_map/pallas_call | solution.py:497
  87.2 3.6 %shard_map.68 = (bf16[2048,1024]{1,0:T(8,128)(2,1)}, bf16[2048,1024]{1,0:T(8,128)(2,1)}, bf16[768,512]{1,0:T(8,128)(2,1)}) custom-call(bf16[2048,1024]{1,0:T(8,128)(2,1)S(1)} %get-tuple-element.6.src_a, bf16[2048,1024]{1,0:T(8,128)(2,1)S(1)} %get-tuple-element.7.src_b, bf16[768,512]{1,0:T(8,128)(2,1)S(1)} %get-tuple-element.8.src_c), custom_call_target="tpu_custom_call" | custom-call | tf_op jit(solution)/shard_map/pallas_call | solution.py:535
